TPU v7x, 32 devices: a whole 2x2x4 slice. The times are simulated.
32 devices in a mesh: sp: 8 (over z, x), tp: 4 (over y, core).
Axes of the slice: x: 2, y: 2, z: 4, core: 2. Of those that a mesh axis runs over, the one named last changes fastest.
Arguments:
- residual: bfloat16 [2048, 2048], P(('sp', 'tp')), may hold values from -6 to 6
- first_query: bfloat16 [2048, 512], P('sp', 'tp'), may hold values from -6 to 6
- second_query: bfloat16 [2048, 512], P('sp', 'tp'), may hold values from -6 to 6
- first_key: bfloat16 [2048, 512], P('sp', 'tp'), may hold values from -6 to 6
- second_key: bfloat16 [2048, 512], P('sp', 'tp'), may hold values from -6 to 6
- values: bfloat16 [2048, 1024], P('sp', 'tp'), may hold values from -6 to 6
- lambdas: float32 [8], P('tp'), may hold values from 0.3 to 0.8
- head_gain: float32 [128], replicated, may hold values from 0.1 to 1.9
- out_weight: bfloat16 [1024, 2048], P('tp'), may hold values from -0.1875 to 0.1875
- norm_gain: float32 [2048], replicated, may hold values from 0.1 to 1.9
- up_weight: bfloat16 [2048, 4096], P('sp', 'tp'), may hold values from -0.125 to 0.125
- down_weight: bfloat16 [4096, 2048], P('tp', 'sp'), may hold values from -0.09375 to 0.09375
Outputs:
- mixed: bfloat16 [2048, 2048], P(('sp', 'tp'))
All inputs are finite; a program needn't handle non-finite values.
Results may differ from a plain program's by a relative error of at most 0.019.
Values may be sent and summed in bfloat16 or wider, within the bound.
A program may use at most 128 MiB of HBM per device.

v0:
```python
import jax
import jax.numpy as jnp
from jax import lax
from jax.sharding import PartitionSpec as P


def rotate(blocked, positions):
    half = blocked.shape[-1] // 2
    inverse = 10000.0 ** (-jnp.arange(0, half, dtype=jnp.float32) * 2.0 / blocked.shape[-1])
    angle = positions[:, None] * inverse[None, :]
    cosine = jnp.cos(angle)[:, None, :]
    sine = jnp.sin(angle)[:, None, :]
    first, second = (blocked[..., :half], blocked[..., half:])
    return jnp.concatenate(
        [first * cosine - second * sine, second * cosine + first * sine], axis=-1
    )


def absorb(state, queries, keys, vals, factor):
    top, total, summed = state
    scores = jnp.einsum("qhe,khe->qhk", queries, keys, preferred_element_type=jnp.float32) * factor
    peak = jnp.maximum(top, jnp.max(scores, axis=-1))
    shrink = jnp.exp(top - peak)
    weights = jnp.exp(scores - peak[..., None])
    total = total * shrink + jnp.sum(weights, axis=-1)
    summed = summed * shrink[..., None] + jnp.einsum(
        "qhk,khe->qhe", weights.astype(jnp.bfloat16), vals, preferred_element_type=jnp.float32
    )
    return (peak, total, summed)


def layer_norm(stream, gain):
    center = stream - jnp.mean(stream, axis=-1, keepdims=True)
    spread = jnp.mean(center * center, axis=-1, keepdims=True)
    return center * lax.rsqrt(spread + 1e-05) * gain


def local(
    residual,
    first_query,
    second_query,
    first_key,
    second_key,
    values,
    lambdas,
    head_gain,
    out_weight,
    norm_gain,
    up_weight,
    down_weight,
):
    local_rows = first_query.shape[0]
    head_count = lambdas.shape[0]
    head_width = first_query.shape[1] // head_count
    value_width = values.shape[1] // head_count
    quarter_rows = local_rows // lax.axis_size("tp")
    factor = head_width ** (-0.5)
    positions = (lax.axis_index("sp") * local_rows + jnp.arange(local_rows)).astype(jnp.float32)

    def prepare(source):
        turned = rotate(
            source.astype(jnp.float32).reshape(local_rows, head_count, head_width), positions
        )
        return turned.astype(jnp.bfloat16)

    query_a, query_b = (prepare(first_query), prepare(second_query))
    key_a = prepare(first_key).reshape(local_rows, head_count * head_width)
    key_b = prepare(second_key).reshape(local_rows, head_count * head_width)
    start_state = (
        jnp.full((local_rows, head_count), -1e30, jnp.float32),
        jnp.zeros((local_rows, head_count), jnp.float32),
        jnp.zeros((local_rows, head_count, value_width), jnp.float32),
    )
    piece_a = lax.all_gather(key_a, "sp", axis=0, tiled=True)
    piece_b = lax.all_gather(key_b, "sp", axis=0, tiled=True)
    piece_v = lax.all_gather(values, "sp", axis=0, tiled=True)
    count = piece_a.shape[0]
    block = 512
    blocks = count // block

    def advance(state, item):
        block_a, block_b, block_v = item
        return (
            (
                absorb(state[0], query_a, block_a, block_v, factor),
                absorb(state[1], query_b, block_b, block_v, factor),
            ),
            None,
        )

    items = (
        piece_a.reshape(blocks, block, head_count, head_width),
        piece_b.reshape(blocks, block, head_count, head_width),
        piece_v.reshape(blocks, block, head_count, value_width),
    )
    state_a, state_b = lax.scan(advance, (start_state, start_state), items)[0]
    diff = state_a[2] / state_a[1][..., None] - lambdas[None, :, None] * (
        state_b[2] / state_b[1][..., None]
    )
    scale = lax.rsqrt(jnp.mean(diff * diff, axis=-1, keepdims=True) + 1e-05)
    flat = (
        (diff * scale * head_gain * 0.8)
        .astype(jnp.bfloat16)
        .reshape(local_rows, head_count * value_width)
    )
    projected = lax.psum(
        jnp.dot(flat, out_weight, preferred_element_type=jnp.float32).astype(jnp.bfloat16), "tp"
    ).astype(jnp.float32)
    stream = lax.all_gather(residual, "tp", axis=0, tiled=True)
    whole = layer_norm(stream.astype(jnp.float32) + projected, norm_gain).astype(jnp.bfloat16)
    own_normed = lax.dynamic_slice_in_dim(
        whole, lax.axis_index("tp") * quarter_rows, quarter_rows, 0
    )
    lifted = jnp.dot(
        whole,
        lax.all_gather(up_weight, "sp", axis=0, tiled=True),
        preferred_element_type=jnp.float32,
    )
    down_full = lax.all_gather(down_weight, "sp", axis=1, tiled=True)
    hidden = jnp.square(jax.nn.relu(lifted)).astype(jnp.bfloat16)
    lowered = lax.psum_scatter(
        jnp.dot(hidden, down_full, preferred_element_type=jnp.float32).astype(jnp.bfloat16),
        "tp",
        scatter_dimension=0,
        tiled=True,
    ).astype(jnp.float32)
    return (own_normed.astype(jnp.float32) + lowered).astype(jnp.bfloat16)


def solution(mesh):
    in_specs = (
        P(("sp", "tp"), None),
        P("sp", "tp"),
        P("sp", "tp"),
        P("sp", "tp"),
        P("sp", "tp"),
        P("sp", "tp"),
        P("tp"),
        P(),
        P("tp", None),
        P(),
        P("sp", "tp"),
        P("tp", "sp"),
    )
    out_specs = P(("sp", "tp"), None)
    return jax.shard_map(local, mesh=mesh, in_specs=in_specs, out_specs=out_specs, check_vma=False)
```

profile of v0, /device:TPU:0, one launch (start us, length us, event | category | flops | bytes accessed | tf_op | source)
XLA Modules:
  0.0 354.3 jit_solution(2607594345238030326)
XLA Ops:
  6.5 0.7 all-gather.7.cloned.1.call-update
  7.3 0.7 all-gather.5.cloned.1.call-update
  8.1 0.9 copy.21
  9.1 0.9 copy.22
  10.0 0.9 copy.23
  11.0 0.9 copy.24
  11.9 0.2 multiply_cosine_fusion
  12.2 34.2 %all_gather.21 = bf16[2048,128]{0,1:T(8,128)(2,1)S(1)} all-gather(bf16[256,128]{0,1:T(8,128)(2,1)S(1)} %bitcast.66), channel_id=1, replica_groups=mesh['sp'=8,'tp'=4] {'sp'}, dimensions={0}, use_global_device_ids=true | all-gather | bytes 589824 | tf_op jit(solution)/shard_map/all_gather | solution.py:75
  46.4 0.4 reshape.137
  46.8 0.9 copy.27
  47.7 31.6 %all_gather.19 = bf16[2048,128]{0,1:T(8,128)(2,1)S(1)} all-gather(bf16[256,128]{0,1:T(8,128)(2,1)S(1)} %bitcast.67), channel_id=1, replica_groups=mesh['sp'=8,'tp'=4] {'sp'}, dimensions={0}, use_global_device_ids=true | all-gather | bytes 589824 | tf_op jit(solution)/shard_map/all_gather | solution.py:74
  79.3 0.4 reshape.131
  79.7 0.9 copy.25
  80.6 2.1 reshape.134
  82.7 42.6 %while.21 = (s32[]{:T(128)}, f32[256,2]{0,1:T(2,128)S(1)}, f32[256,2]{0,1:T(2,128)}, f32[256,2,128]{0,2,1:T(8,128)}, f32[256,2]{0,1:T(2,128)S(1)}, /*index=5*/f3...) while((s32[]{:T(128)}, f32[256,2]{0,1:T(2,128)S(1)}, ...), condition=%wide.region_5.6_spmd.clone, body=%wide.region_0.5_spmd.clone.sunk | while | flops 204870656 | bytes 9381043 | solution.py:96
  82.7 1.3 fusion.60
  84.0 0.2 fusion.65
  84.2 1.3 fusion.62
  85.5 0.2 fusion.64
  85.6 0.6 fusion.66
  86.3 1.8 constant_dynamic-slice_fusion.2
  88.1 1.1 copy.32
  89.2 1.7 fusion.68
  90.9 1.0 fusion.67
  92.0 1.3 fusion.60
  93.2 0.2 fusion.65
  93.4 1.3 fusion.62
  94.7 0.2 fusion.64
  94.9 1.3 fusion.66
  96.2 1.8 constant_dynamic-slice_fusion.2
  98.0 1.1 copy.32
  99.1 2.0 fusion.68
  101.1 2.0 fusion.67
  103.1 1.3 fusion.60
  104.4 0.2 fusion.65
  104.5 1.3 fusion.62
  105.8 0.2 fusion.64
  106.0 1.3 fusion.66
  107.3 1.8 constant_dynamic-slice_fusion.2
  109.1 1.1 copy.32
  110.2 2.0 fusion.68
  112.2 2.0 fusion.67
  114.2 1.3 fusion.60
  115.7 1.3 fusion.62
  116.9 0.2 fusion.64
  117.1 1.3 fusion.66
  118.4 1.8 constant_dynamic-slice_fusion.2
  120.3 1.1 copy.32
  121.4 2.0 fusion.68
  123.4 2.0 fusion.67
  125.3 1.2 multiply_reduce_fusion.1
  126.5 0.7 multiply_convert_fusion.1
  127.3 1.4 convolution_convert_fusion.1
  128.8 0.5 all-gather.11.cloned.1.call-update
  129.4 0.5 all-gather.9.cloned.1.call-update
  130.0 35.5 %all-reduce.2.cloned.1.call-done = bf16[256,2048]{1,0:T(8,128)(2,1)} async-done(((bf16[256,2048]{1,0:T(8,128)(2,1)}), bf16[256,2048]{1,0:T(8,128)(2,1)}) %all-reduce.2.cloned.1.call-update) | async-done | bytes 1048592 | tf_op jit(solution)/shard_map/psum | solution.py:106
  165.4 2.0 fusion.25
  167.5 0.5 multiply_reduce_fusion
  168.0 0.5 multiply_convert_fusion
  168.5 74.0 %all-gather.11.cloned.1.call-done = bf16[1024,2048]{1,0:T(8,128)(2,1)} async-done(((bf16[1024,256]{1,0:T(8,128)(2,1)}), bf16[1024,2048]{1,0:T(8,128)(2,1)}) %all-gather.11.cloned.1.call-update) | async-done | bytes 4194320 | tf_op jit(solution)/shard_map/all_gather | solution.py:119
  242.5 73.0 %all-gather.9.cloned.1.call-done = bf16[2048,1024]{1,0:T(8,128)(2,1)} async-done(((bf16[256,1024]{1,0:T(8,128)(2,1)}), bf16[2048,1024]{1,0:T(8,128)(2,1)}) %all-gather.9.cloned.1.call-update) | async-done | bytes 4194320 | tf_op jit(solution)/shard_map/all_gather | solution.py:116
  315.5 6.8 %convolution_convert_fusion = bf16[256,2048]{1,0:T(8,128)(2,1)} fusion(bf16[1024,2048]{1,0:T(8,128)(2,1)} %all-gather.11.cloned.1.call-done, bf16[256,2048]{1,0:T(8,128)(2,1)S(1)} %multiply_convert_fusion, bf16[2048,1024]{1,0:T(8,128)(2,1)} %all-gather.9.cloned.1.call-done), kind=kOutput, calls=%fused_computation.37 | convolution fusion | flops 2148794368 | bytes 10485760 | tf_op jit(solution)/shard_map/dot_general | solution.py:122
  322.3 23.5 %reduce-scatter.2.cloned.1.call-done = bf16[64,2048]{1,0:T(8,128)(2,1)} async-done(((bf16[256,2048]{1,0:T(8,128)(2,1)}), bf16[64,2048]{1,0:T(8,128)(2,1)}) %reduce-scatter.2.cloned.1.call-update) | async-done | bytes 262160 | tf_op jit(solution)/shard_map/reduce_scatter | solution.py:121
  345.8 1.7 add_convert_fusion
  (58 shorter events, 0.7 us)
Async XLA Ops:
  6.5 120.7 %copy-start = (bf16[256,2048]{1,0:T(8,128)(2,1)S(1)}, bf16[256,2048]{1,0:T(8,128)(2,1)}, u32[]{:S(2)}) copy-start(bf16[256,2048]{1,0:T(8,128)(2,1)} %param.22) | copy-start | bytes 3145732
  6.5 74.1 %all-gather.7.cloned.1.call-start = ((), (), s32[]{:S(2)}) async-start(), calls=%async_computation.2 | async-start | bytes 1179648 | tf_op jit(solution)/shard_map/all_gather | solution.py:76
  7.3 122.7 %all-gather.5.cloned.1.call-start = ((), (), s32[]{:S(2)}) async-start(), calls=%async_computation.1 | async-start | bytes 1310720 | tf_op jit(solution)/shard_map/all_gather | solution.py:109
  8.0 157.4 %all-reduce.2.cloned.1.call-start = ((), (), s32[]{:S(2)}) async-start(), calls=%async_computation.3 | async-start | bytes 2097152 | tf_op jit(solution)/shard_map/psum | solution.py:106
  86.3 4.7 %copy-start.3 = (f32[256,2]{0,1:T(2,128)S(1)}, f32[256,2]{0,1:T(2,128)}, u32[]{:S(2)}) copy-start(f32[256,2]{0,1:T(2,128)} %get-tuple-element.265) | copy-start | bytes 6148 | tf_op jit(solution)/shard_map/while
  96.2 4.9 %copy-start.3 = (f32[256,2]{0,1:T(2,128)S(1)}, f32[256,2]{0,1:T(2,128)}, u32[]{:S(2)}) copy-start(f32[256,2]{0,1:T(2,128)} %get-tuple-element.265) | copy-start | bytes 6148 | tf_op jit(solution)/shard_map/while
  107.3 4.9 %copy-start.3 = (f32[256,2]{0,1:T(2,128)S(1)}, f32[256,2]{0,1:T(2,128)}, u32[]{:S(2)}) copy-start(f32[256,2]{0,1:T(2,128)} %get-tuple-element.265) | copy-start | bytes 6148 | tf_op jit(solution)/shard_map/while
  118.4 4.9 %copy-start.3 = (f32[256,2]{0,1:T(2,128)S(1)}, f32[256,2]{0,1:T(2,128)}, u32[]{:S(2)}) copy-start(f32[256,2]{0,1:T(2,128)} %get-tuple-element.265) | copy-start | bytes 6148 | tf_op jit(solution)/shard_map/while
  128.7 113.7 %all-gather.11.cloned.1.call-start = ((), (), s32[]{:S(2)}) async-start(), calls=%async_computation.5 | async-start | bytes 4718592 | tf_op jit(solution)/shard_map/all_gather | solution.py:119
  129.3 186.1 %all-gather.9.cloned.1.call-start = ((), (), s32[]{:S(2)}) async-start(), calls=%async_computation.4 | async-start | bytes 4718592 | tf_op jit(solution)/shard_map/all_gather | solution.py:116
  129.4 38.6 %copy-start.4 = (f32[2048]{0:T(1024)S(1)}, f32[2048]{0:T(1024)}, u32[]{:S(2)}) copy-start(f32[2048]{0:T(1024)} %param.23) | copy-start | bytes 24580
  129.9 215.9 %reduce-scatter.2.cloned.1.call-start = ((), (), s32[]{:S(2)}) async-start(), calls=%async_computation.6 | async-start | bytes 1310720 | tf_op jit(solution)/shard_map/reduce_scatter | solution.py:121
  130.0 37.5 %copy-start.1 = (bf16[256,2048]{1,0:T(8,128)(2,1)S(1)}, bf16[256,2048]{1,0:T(8,128)(2,1)}, u32[]{:S(2)}) copy-start(bf16[256,2048]{1,0:T(8,128)(2,1)} %all-gather.5.cloned.1.call-done) | copy-start | bytes 3145732
  165.4 2.0 copy-start.2
Sparse Core Ops, SparseCore 0:
  9.5 45.4 all-gather.6
  56.5 15.4 all-gather.4
  128.9 36.5 all-reduce.1
  167.3 75.0 all-gather.10
  244.4 70.9 all-gather.8
  322.4 23.2 reduce-scatter.1
where the time goes:
time: 355 us; the launch traced here: 354 us
  waiting for transfers between devices  208 us (59%)
  blocking collectives  65.8 us (19%)
  matrix products  33 us (9%)
  local copies, waits for them, and re-layouts  20.2 us (6%)
  between operations  13.7 us (4%)
  other arithmetic  12.9 us (4%)
    all_gather x1, waiting for transfers between devices, local(): down_full = lax.all_gather(down_weight, 'sp', axis=1, tiled=True)  74 us
    all_gather x1, waiting for transfers between devices, local(): lax.all_gather(up_weight, 'sp', axis=0, tiled=True)  73 us
    psum x1, waiting for transfers between devices, local(): lax.psum(jnp.dot(flat, out_weight, preferred_element_type=jnp.float32).as...  35.5 us
    all_gather x1, blocking collectives, local(): piece_b = lax.all_gather(key_b, 'sp', axis=0, tiled=True)  34.2 us
    all_gather x1, blocking collectives, local(): piece_a = lax.all_gather(key_a, 'sp', axis=0, tiled=True)  31.6 us
    reduce_scatter x1, waiting for transfers between devices, local(): lax.psum_scatter(jnp.dot(hidden, down_full, preferred_element_type=jnp.fl...  23.5 us
    dot_general x8, matrix products, absorb(): jnp.einsum('qhk,khe->qhe', weights.astype(jnp.bfloat16), vals, preferred_...  14.6 us
    dynamic_slice x8, local copies, waits for them, and re-layouts, local(): state_a, state_b = lax.scan(advance, (start_state, start_state), items)[0]  11.8 us
  transfers between devices with their start and end apart: 6, of which 4 were waited for; matrix products, arithmetic and copies ran while one was open for 16% of the time, Pallas kernels for 0%

commit v1 on v0

--- a/solution.py
+++ b/solution.py
@@ -1,6 +1,10 @@
+import functools
+
 import jax
 import jax.numpy as jnp
 from jax import lax
+from jax.experimental import pallas as pl
+from jax.experimental.pallas import tpu as pltpu
 from jax.sharding import PartitionSpec as P
 
 
@@ -127,6 +131,313 @@
     return (own_normed.astype(jnp.float32) + lowered).astype(jnp.bfloat16)
 
 
+BF = jnp.bfloat16
+F32 = jnp.float32
+VMEM_BUDGET = 40 * 2**20
+
+
+def prep_kernel(heads, qa_ref, qb_ref, ka_ref, kb_ref, v_ref, cos_ref, sin_ref, qm_ref, kv_ref):
+    rows, width = qa_ref.shape
+    head_width = width // heads
+    half = head_width // 2
+    lane = lax.broadcasted_iota(jnp.int32, (rows, width), 1)
+    low = (lane % head_width) < half
+    cos, sin = cos_ref[...], sin_ref[...]
+
+    def turn(ref):
+        x = ref[...].astype(F32)
+        other = jnp.where(low, pltpu.roll(x, width - half, 1), pltpu.roll(x, half, 1))
+        return x * cos + other * sin
+
+    for which, ref in enumerate((qa_ref, qb_ref)):
+        q = turn(ref).astype(BF).astype(F32) * head_width ** (-0.5)
+        for h in range(heads):
+            own = (lane // head_width) == h
+            qm_ref[which, h * rows : (h + 1) * rows, :] = jnp.where(own, q, 0.0).astype(BF)
+    kv_ref[:, :width] = turn(ka_ref).astype(BF)
+    kv_ref[:, width : 2 * width] = turn(kb_ref).astype(BF)
+    kv_ref[:, 2 * width :] = v_ref[...]
+
+
+def layer_kernel(
+    n, nt, heads,
+    qm, kv0, lam, hgain, ow0, res0, ngain, up0, dn0,
+    out,
+    kv, up, dn, ow, res, flat, normed, lifted, hidden, part, mine, got,
+    top, total, summed, send, recv,
+):
+    s = lax.axis_index("sp")
+    t = lax.axis_index("tp")
+    rows, kv_width = kv0.shape
+    width = qm.shape[2]
+    value_width = (kv_width - 2 * width) // heads
+    depth = up0.shape[0]
+    units = up0.shape[1]
+    model = ow0.shape[1]
+    piece = res0.shape[0]
+    mid = n // 2
+    odd = s % 2
+    place = (1 - odd) * (s // 2) + odd * (n - 1 - s // 2)
+
+    def at_place(p):
+        p = p % n
+        hi = p // mid
+        return (1 - hi) * (2 * p) + hi * (2 * (n - 1 - p) + 1)
+
+    def owner(slot):
+        return at_place(place - slot + n)
+
+    right = {"sp": at_place(place + 1)}
+    left = {"sp": at_place(place + n - 1)}
+    mates = [{"tp": (t + d) % nt} for d in range(1, nt)]
+    barrier = pltpu.get_barrier_semaphore()
+    for peer in [right, left] + mates:
+        pl.semaphore_signal(barrier, inc=1, device_id=peer, device_id_type=pl.DeviceIdType.MESH)
+    pl.semaphore_wait(barrier, nt + 1)
+
+    copies = []
+
+    def remote(src, dst, peer):
+        i = len(copies)
+        c = pltpu.make_async_remote_copy(
+            src_ref=src, dst_ref=dst, send_sem=send.at[i], recv_sem=recv.at[i],
+            device_id=peer, device_id_type=pl.DeviceIdType.MESH,
+        )
+        c.start()
+        copies.append(c)
+        return c
+
+    def ring(own, buf, k, lo=0, hi=None):
+        size = own.shape[0]
+        hi = size if hi is None else hi
+        a, b = (lo, hi), (lo, hi)
+        if k == mid:
+            a, b = (0, size // 2), (size // 2, size)
+        cut_a, cut_b = pl.ds(a[0], a[1] - a[0]), pl.ds(b[0], b[1] - b[0])
+        src_a = own.at[cut_a] if k == 1 else buf.at[k - 1, cut_a]
+        src_b = own.at[cut_b] if k == 1 else buf.at[n - k + 1, cut_b]
+        return [
+            remote(src_a, buf.at[k, cut_a], right),
+            remote(src_b, buf.at[n - k, cut_b], left),
+        ]
+
+    def arrive(group):
+        for c in group:
+            c.wait_recv()
+
+    def absorb(block):
+        for which in range(2):
+            keys = block[:, which * width : (which + 1) * width]
+            for h in range(heads):
+                at = which * heads + h
+                scores = lax.dot_general(
+                    keys, qm[which, h * rows : (h + 1) * rows, :],
+                    (((1,), (1,)), ((), ())), preferred_element_type=F32,
+                )
+                old = top[at]
+                peak = jnp.maximum(old, jnp.max(scores, axis=0, keepdims=True))
+                shrink = jnp.exp(old - peak)
+                e = jnp.exp(scores - peak)
+                top[at] = peak
+                total[at] = total[at] * shrink + jnp.sum(e, axis=0, keepdims=True)
+                first = 2 * width + h * value_width
+                vals = block[:, first : first + value_width]
+                summed[at] = summed[at] * shrink + lax.dot_general(
+                    vals, e.astype(BF), (((0,), (0,)), ((), ())), preferred_element_type=F32
+                )
+
+    def absorb_pair(k):
+        def body(i, carry):
+            absorb(kv[k + i * (n - 2 * k)])
+            return carry
+
+        lax.fori_loop(0, 2, body, 0)
+
+    cuts = [(i * depth // mid, (i + 1) * depth // mid) for i in range(mid)]
+    got_kv = ring(kv0, kv, 1)
+    got_res = [remote(res0, res.at[t], m) for m in mates]
+    got_ow = [remote(ow0, ow.at[d], m) for d, m in enumerate(mates)]
+    got_up = ring(up0, up, 1, *cuts[0])
+    top[...] = jnp.full(top.shape, -1e30, F32)
+    total[...] = jnp.zeros(total.shape, F32)
+    summed[...] = jnp.zeros(summed.shape, F32)
+    res[t] = res0[...]
+    absorb(kv0[...])
+    for k in range(1, mid):
+        arrive(got_kv)
+        got_kv = ring(kv0, kv, k + 1)
+        got_up += ring(up0, up, 1, *cuts[k])
+        if k == mid - 1:
+            got_dn = ring(dn0, dn, 1)
+        absorb_pair(k)
+    arrive(got_kv)
+    absorb(kv[mid])
+
+    for h in range(heads):
+        a = summed[h] / total[h]
+        b = summed[heads + h] / total[heads + h]
+        diff = a - lam[h] * b
+        scale = lax.rsqrt(jnp.mean(diff * diff, axis=0, keepdims=True) + 1e-05)
+        done = diff * scale * hgain[...] * 0.8
+        flat[0, :, h * value_width : (h + 1) * value_width] = done.T.astype(BF)
+
+    arrive(got_up)
+    got_up = ring(up0, up, 2)
+    got_flat = [remote(flat.at[0], flat.at[d + 1], m) for d, m in enumerate(mates)]
+    arrive(got_dn)
+    got_dn = ring(dn0, dn, 2)
+    arrive(got_res + got_ow + got_flat)
+
+    chunk = piece
+    def norm_rows(q, carry):
+        rows_at = pl.ds(pl.multiple_of(q * chunk, chunk), chunk)
+        stream = res[q].astype(F32) + jnp.dot(flat[0, rows_at, :], ow0[...], preferred_element_type=F32)
+        for d in range(1, nt):
+            stream += jnp.dot(flat[d, rows_at, :], ow[d - 1], preferred_element_type=F32)
+        center = stream - jnp.mean(stream, axis=-1, keepdims=True)
+        spread = jnp.mean(center * center, axis=-1, keepdims=True)
+        row = (center * lax.rsqrt(spread + 1e-05) * ngain[...]).astype(BF)
+        for i in range(n):
+            normed[i, q] = row[:, i * depth : (i + 1) * depth]
+        return carry
+
+    lax.fori_loop(0, nt, norm_rows, 0)
+
+    def lift(block, slot):
+        x = normed[owner(slot)].reshape(rows, depth)
+        return jnp.dot(x, block, preferred_element_type=F32)
+
+    def lift_pair(k):
+        def body(i, carry):
+            slot = k + i * (n - 2 * k)
+            lifted[...] += lift(up[slot], slot)
+            return carry
+
+        lax.fori_loop(0, 2, body, 0)
+
+    lifted[...] = lift(up0[...], 0)
+    lift_pair(1)
+    for k in range(2, mid):
+        arrive(got_up)
+        got_up = ring(up0, up, k + 1)
+        lift_pair(k)
+        arrive(got_dn)
+        got_dn = ring(dn0, dn, k + 1)
+    arrive(got_up)
+    h = jnp.maximum(lifted[...] + lift(up[mid], mid), 0.0)
+    hidden[...] = (h * h).astype(BF)
+
+    waits = []
+
+    def lower(block, slot):
+        y = jnp.dot(hidden[...], block, preferred_element_type=F32).reshape(nt, piece, depth)
+        mine[slot] = y
+        part[slot] = y.astype(BF)
+
+    def share(slot):
+        waits.append((slot, [
+            remote(part.at[slot, (t + d) % nt], got.at[slot, d - 1], mates[d - 1])
+            for d in range(1, nt)
+        ]))
+
+    def finish(slot, group):
+        arrive(group)
+        who = owner(slot)
+        y = normed[who, t].astype(F32) + mine[slot, t]
+        for d in range(nt - 1):
+            y += got[slot, d].astype(F32)
+        out[:, pl.ds(pl.multiple_of(who * depth, depth), depth)] = y.astype(BF)
+
+    lower(dn0[...], 0)
+    for k in range(1, mid):
+        lower(dn[k], k)
+        share(0 if k == 1 else n - k + 1)
+        lower(dn[n - k], n - k)
+        share(k)
+    share(mid + 1)
+    for slot, group in waits[:-2]:
+        finish(slot, group)
+    arrive(got_dn)
+    lower(dn[mid], mid)
+    for slot, group in waits[-2:]:
+        finish(slot, group)
+    share(mid)
+    finish(*waits[-1])
+    for c in copies:
+        c.wait_send()
+
+
+def fused(n, nt, residual, first_query, second_query, first_key, second_key, values,
+          lambdas, head_gain, out_weight, norm_gain, up_weight, down_weight):
+    rows, width = first_query.shape
+    heads = lambdas.shape[0]
+    head_width = width // heads
+    value_width = values.shape[1] // heads
+    half = head_width // 2
+    depth, units = up_weight.shape
+    model = out_weight.shape[1]
+    piece = residual.shape[0]
+    positions = (lax.axis_index("sp") * rows + jnp.arange(rows)).astype(F32)
+    inverse = 10000.0 ** (-jnp.arange(0, half, dtype=F32) * 2.0 / head_width)
+    angle = positions[:, None] * inverse[None, :]
+    cosine, sine = jnp.cos(angle), jnp.sin(angle)
+    cosine = jnp.concatenate([cosine] * (2 * heads), axis=1)
+    sine = jnp.concatenate([-sine, sine] * heads, axis=1)
+    kv_width = 2 * width + heads * value_width
+    qm, kv0 = pl.pallas_call(
+        functools.partial(prep_kernel, heads),
+        out_shape=(
+            jax.ShapeDtypeStruct((2, heads * rows, width), BF),
+            jax.ShapeDtypeStruct((rows, kv_width), BF),
+        ),
+        name="prepare",
+    )(first_query, second_query, first_key, second_key, values, cosine, sine)
+    vmem = pl.BlockSpec(memory_space=pltpu.VMEM)
+    smem = pl.BlockSpec(memory_space=pltpu.SMEM)
+    mid = n // 2
+    count = 2 * mid + 2 * (2 * mid - 1) + 2 * mid + 3 * (nt - 1) + n * (nt - 1)
+    maps = 2 * heads
+    return pl.pallas_call(
+        functools.partial(layer_kernel, n, nt, heads),
+        out_shape=jax.ShapeDtypeStruct((piece, model), BF),
+        in_specs=[vmem, vmem, smem] + [vmem] * 6,
+        out_specs=vmem,
+        scratch_shapes=[
+            pltpu.VMEM((n, rows, kv_width), BF),
+            pltpu.VMEM((n, depth, units), BF),
+            pltpu.VMEM((n, units, depth), BF),
+            pltpu.VMEM((nt - 1,) + out_weight.shape, BF),
+            pltpu.VMEM((nt, piece, model), BF),
+            pltpu.VMEM((nt, rows, heads * value_width), BF),
+            pltpu.VMEM((n, nt, piece, depth), BF),
+            pltpu.VMEM((rows, units), F32),
+            pltpu.VMEM((rows, units), BF),
+            pltpu.VMEM((n, nt, piece, depth), BF),
+            pltpu.VMEM((n, nt, piece, depth), F32),
+            pltpu.VMEM((n, nt - 1, piece, depth), BF),
+            pltpu.VMEM((maps, 1, rows), F32),
+            pltpu.VMEM((maps, 1, rows), F32),
+            pltpu.VMEM((maps, value_width, rows), F32),
+            pltpu.SemaphoreType.DMA((count,)),
+            pltpu.SemaphoreType.DMA((count,)),
+        ],
+        compiler_params=pltpu.CompilerParams(
+            collective_id=0, has_side_effects=True, vmem_limit_bytes=60 * 2**20
+        ),
+        name="layer",
+    )(qm, kv0, lambdas, head_gain.reshape(-1, 1), out_weight, residual,
+      norm_gain.reshape(1, -1), up_weight, down_weight)
+
+
+def choose(*args):
+    n, nt = lax.axis_size("sp"), lax.axis_size("tp")
+    gathered = n * sum(a.size * a.dtype.itemsize for a in (args[3], args[4], args[5], args[10], args[11]))
+    gathered += nt * sum(a.size * a.dtype.itemsize for a in (args[0], args[8]))
+    if n % 2 == 0 and n >= 6 and 2 * gathered <= VMEM_BUDGET:
+        return fused(n, nt, *args)
+    return local(*args)
+
+
 def solution(mesh):
     in_specs = (
         P(("sp", "tp"), None),
@@ -143,4 +454,4 @@
         P("tp", "sp"),
     )
     out_specs = P(("sp", "tp"), None)
-    return jax.shard_map(local, mesh=mesh, in_specs=in_specs, out_specs=out_specs, check_vma=False)
+    return jax.shard_map(choose, mesh=mesh, in_specs=in_specs, out_specs=out_specs, check_vma=False)

time: 355 us -> 127 us (0.36)
  waiting for transfers between devices: 208 us -> 0 us
  Pallas kernels: 0 us -> 122 us
  blocking collectives: 65.8 us -> 0 us
  matrix products: 33 us -> 0 us
  local copies, waits for them, and re-layouts: 20.2 us -> 3.05 us
  between operations: 13.7 us -> 0.02 us
  other arithmetic: 12.9 us -> 1.52 us
    all_gather x4 -> x0, waiting for transfers between devices: 147 us -> none  [the longest x1 74 us: local(): down_full = lax.all_gather(down_weight, 'sp', axis=1, tiled=True)]
    pallas_call x0 -> x2, Pallas kernels: none -> 122 us  [the longest x1 120 us: fused(): pl.pallas_call(functools.partial(layer_kernel, n, nt, heads), out_shape=j...]
    all_gather x2 -> x0, blocking collectives: 65.8 us -> none  [the longest x1 34.2 us: local(): piece_b = lax.all_gather(key_b, 'sp', axis=0, tiled=True)]
    psum x1 -> x0, waiting for transfers between devices: 35.5 us -> none  [local(): lax.psum(jnp.dot(flat, out_weight, preferred_element_type=jnp.float32).as...]
    dot_general x18 -> x0, matrix products: 33 us -> none  [the longest x8 14.6 us: absorb(): jnp.einsum('qhk,khe->qhe', weights.astype(jnp.bfloat16), vals, preferred_...]
    reduce_scatter x1 -> x0, waiting for transfers between devices: 23.5 us -> none  [local(): lax.psum_scatter(jnp.dot(hidden, down_full, preferred_element_type=jnp.fl...]
    dynamic_slice x8 -> x0, local copies, waits for them, and re-layouts: 11.8 us -> none  [local(): state_a, state_b = lax.scan(advance, (start_state, start_state), items)[0]]
    reshape x7 -> x1, local copies, waits for them, and re-layouts: 6.64 us -> 0.73 us  [fused(): head_gain.reshape(-1, 1)]
  transfers between devices with their start and end apart: 6 -> 0, of which waited for: 4 -> 0; matrix products, arithmetic and copies ran while one was open for 16% -> 0% of each run, Pallas kernels for 0% -> 0%
where the time goes in v1:
time: 127 us
  Pallas kernels  122 us (96%)
  local copies, waits for them, and re-layouts  3.05 us (2%)
  other arithmetic  1.52 us (1%)
    pallas_call x1, Pallas kernels, fused(): pl.pallas_call(functools.partial(layer_kernel, n, nt, heads), out_shape=j...  120 us

profile of v1, /device:TPU:0, one launch (start us, length us, event | category | flops | bytes accessed | tf_op | source)
XLA Modules:
  0.0 126.6 jit_solution(13159178987754984186)
XLA Ops:
  0.0 0.5 fusion
  0.6 1.0 pad_maximum_fusion
  1.5 2.1 %prepare.1 = (bf16[2,512,128]{2,1,0:T(8,128)(2,1)}, bf16[256,512]{1,0:T(8,128)(2,1)}) custom-call(bf16[256,128]{1,0:T(8,128)(2,1)} %qa_ref.1, bf16[256,128]{1,0:T(8,128)(2,1)} %qb_ref.1, bf16[256,128]{1,0:T(8,128)(2,1)} %ka_ref.1, bf16[256,128]{1,0:T(8,128)(2,1)} %kb_ref.1, bf16[256,256]{1,0:T(8,128)(2,1)} %v_ref.1, f32[256,128]{1,0:T(8,128)} %get-tuple-element.12.cos_ref, ...), custom_call_target="tpu_custom_call" | custom-call | tf_op jit(solution)/shard_map/prepare/pallas_call | solution.py:387
  3.7 0.0 copy-start
  3.7 0.7 copy-done
  4.3 0.7 copy.15.hgain
  5.1 119.9 %layer.1 = bf16[64,2048]{1,0:T(8,128)(2,1)} custom-call(bf16[2,512,128]{2,1,0:T(8,128)(2,1)} %get-tuple-element.7.qm, bf16[256,512]{1,0:T(8,128)(2,1)} %get-tuple-element.8.kv0, f32[2]{0:T(128)} %lam.1, f32[128,1]{1,0:T(8,128)} %copy.15.hgain, bf16[256,2048]{1,0:T(8,128)(2,1)} %ow0.1, bf16[64,2048]{1,0:T(8,128)(2,1)} %res0.1, f32[1,2048]{1,0:T(1,128)} %bitcast.2, ...), custom_call_target="tpu_custom_call" | custom-call | tf_op jit(solution)/shard_map/layer/pallas_call | solution.py:400
  125.0 1.7 %copy.17 = bf16[64,2048]{1,0:T(8,128)(2,1)} copy(bf16[64,2048]{1,0:T(8,128)(2,1)} %layer.1) | data formatting | bytes 524288
  (2 shorter events, 0.0 us)
Async XLA Ops:
  3.7 0.7 copy-start

commit v2 on v1

--- a/solution.py
+++ b/solution.py
@@ -136,34 +136,11 @@
 VMEM_BUDGET = 40 * 2**20
 
 
-def prep_kernel(heads, qa_ref, qb_ref, ka_ref, kb_ref, v_ref, cos_ref, sin_ref, qm_ref, kv_ref):
-    rows, width = qa_ref.shape
-    head_width = width // heads
-    half = head_width // 2
-    lane = lax.broadcasted_iota(jnp.int32, (rows, width), 1)
-    low = (lane % head_width) < half
-    cos, sin = cos_ref[...], sin_ref[...]
-
-    def turn(ref):
-        x = ref[...].astype(F32)
-        other = jnp.where(low, pltpu.roll(x, width - half, 1), pltpu.roll(x, half, 1))
-        return x * cos + other * sin
-
-    for which, ref in enumerate((qa_ref, qb_ref)):
-        q = turn(ref).astype(BF).astype(F32) * head_width ** (-0.5)
-        for h in range(heads):
-            own = (lane // head_width) == h
-            qm_ref[which, h * rows : (h + 1) * rows, :] = jnp.where(own, q, 0.0).astype(BF)
-    kv_ref[:, :width] = turn(ka_ref).astype(BF)
-    kv_ref[:, width : 2 * width] = turn(kb_ref).astype(BF)
-    kv_ref[:, 2 * width :] = v_ref[...]
-
-
 def layer_kernel(
     n, nt, heads,
-    qm, kv0, lam, hgain, ow0, res0, ngain, up0, dn0,
+    qa, qb, ka, kb, v0, inverse, lam, hgain, ow0, res0, ngain, up0, dn0,
     out,
-    kv, up, dn, ow, res, flat, normed, lifted, hidden, part, mine, got,
+    qm, kv0, kv, up, dn, ow, res, flat, normed, lifted, hidden, part, mine, got,
     top, total, summed, send, recv,
 ):
     s = lax.axis_index("sp")
@@ -207,19 +184,28 @@
         copies.append(c)
         return c
 
-    def ring(own, buf, k, lo=0, hi=None):
+    own_of = {"kv": (kv0, kv), "up": (up0, up), "dn": (dn0, dn)}
+    groups = {}
+
+    def issue(name, k, *which):
+        own, buf = own_of[name]
         size = own.shape[0]
-        hi = size if hi is None else hi
-        a, b = (lo, hi), (lo, hi)
-        if k == mid:
-            a, b = (0, size // 2), (size // 2, size)
-        cut_a, cut_b = pl.ds(a[0], a[1] - a[0]), pl.ds(b[0], b[1] - b[0])
-        src_a = own.at[cut_a] if k == 1 else buf.at[k - 1, cut_a]
-        src_b = own.at[cut_b] if k == 1 else buf.at[n - k + 1, cut_b]
-        return [
-            remote(src_a, buf.at[k, cut_a], right),
-            remote(src_b, buf.at[n - k, cut_b], left),
-        ]
+        for i in which:
+            if k > 1:
+                ready(name, k - 1, i)
+            a = pl.ds(i * (size // 2), size // 2)
+            b = pl.ds((1 - i) * (size // 2), size // 2)
+            src_a = own.at[a] if k == 1 else buf.at[k - 1, a]
+            src_b = own.at[b] if k == 1 else buf.at[n - k + 1, b]
+            groups[name, k, i] = [
+                remote(src_a, buf.at[k, a], right),
+                remote(src_b, buf.at[n - k, b], left),
+            ]
+
+    def ready(name, k, *which):
+        for i in which:
+            arrive(groups[name, k, i])
+            groups[name, k, i] = []
 
     def arrive(group):
         for c in group:
@@ -253,24 +239,56 @@
 
         lax.fori_loop(0, 2, body, 0)
 
-    cuts = [(i * depth // mid, (i + 1) * depth // mid) for i in range(mid)]
-    got_kv = ring(kv0, kv, 1)
-    got_res = [remote(res0, res.at[t], m) for m in mates]
-    got_ow = [remote(ow0, ow.at[d], m) for d, m in enumerate(mates)]
-    got_up = ring(up0, up, 1, *cuts[0])
+    partner = {"tp": t + 1 - 2 * (t % 2)}
+    issue("up", 1, 0)
+    across = range(2, nt, 2)
+    far = [
+        (d, [remote(res0, res.at[t], {"tp": (t + d) % nt}), remote(ow0, ow.at[t], {"tp": (t + d) % nt})])
+        for d in across
+    ]
+    near = [remote(res0, res.at[t], partner), remote(ow0, ow.at[t], partner)]
+    head_width = width // heads
+    half = head_width // 2
+    lane = lax.broadcasted_iota(jnp.int32, (rows, width), 1)
+    low = (lane % head_width) < half
+    position = (lax.broadcasted_iota(jnp.int32, (rows, width), 0) + s * rows).astype(F32)
+    angle = position * inverse[...]
+    cos = jnp.cos(angle)
+    sin = jnp.sin(angle)
+    sin = jnp.where(low, -sin, sin)
+
+    def turn(ref):
+        x = ref[...].astype(F32)
+        other = jnp.where(low, pltpu.roll(x, width - half, 1), pltpu.roll(x, half, 1))
+        return x * cos + other * sin
+
+    kv0[:, 2 * width :] = v0[...]
+    kv0[:, :width] = turn(ka).astype(BF)
+    kv0[:, width : 2 * width] = turn(kb).astype(BF)
+    for which, ref in enumerate((qa, qb)):
+        q = turn(ref).astype(BF).astype(F32) * head_width ** (-0.5)
+        for h in range(heads):
+            own = (lane // head_width) == h
+            qm[which, h * rows : (h + 1) * rows, :] = jnp.where(own, q, 0.0).astype(BF)
+    issue("kv", 1, 0, 1)
+    issue("up", 1, 1)
     top[...] = jnp.full(top.shape, -1e30, F32)
     total[...] = jnp.zeros(total.shape, F32)
     summed[...] = jnp.zeros(summed.shape, F32)
     res[t] = res0[...]
     absorb(kv0[...])
+    fillers = [("dn", 1, 0), ("dn", 1, 1), ("up", 2, 0, 1)]
     for k in range(1, mid):
-        arrive(got_kv)
-        got_kv = ring(kv0, kv, k + 1)
-        got_up += ring(up0, up, 1, *cuts[k])
-        if k == mid - 1:
-            got_dn = ring(dn0, dn, 1)
+        issue("kv", k + 1, 0)
+        ready("kv", k, 1)
+        if k + 1 < mid:
+            issue("kv", k + 1, 1)
+        if fillers:
+            issue(*fillers.pop(0))
         absorb_pair(k)
-    arrive(got_kv)
+    for filler in fillers:
+        issue(*filler)
+    ready("kv", mid, 0)
     absorb(kv[mid])
 
     for h in range(heads):
@@ -278,22 +296,23 @@
         b = summed[heads + h] / total[heads + h]
         diff = a - lam[h] * b
         scale = lax.rsqrt(jnp.mean(diff * diff, axis=0, keepdims=True) + 1e-05)
-        done = diff * scale * hgain[...] * 0.8
-        flat[0, :, h * value_width : (h + 1) * value_width] = done.T.astype(BF)
-
-    arrive(got_up)
-    got_up = ring(up0, up, 2)
+        done = (diff * scale).T * hgain[...] * 0.8
+        flat[0, :, h * value_width : (h + 1) * value_width] = done.astype(BF)
+
     got_flat = [remote(flat.at[0], flat.at[d + 1], m) for d, m in enumerate(mates)]
-    arrive(got_dn)
-    got_dn = ring(dn0, dn, 2)
-    arrive(got_res + got_ow + got_flat)
+    issue("dn", 2, 0, 1)
+    for d, pair in far:
+        arrive(pair)
+        there = (t + nt - d) % nt
+        near += [remote(res.at[there], res.at[there], partner), remote(ow.at[there], ow.at[there], partner)]
+    arrive(near + got_flat)
 
     chunk = piece
     def norm_rows(q, carry):
         rows_at = pl.ds(pl.multiple_of(q * chunk, chunk), chunk)
         stream = res[q].astype(F32) + jnp.dot(flat[0, rows_at, :], ow0[...], preferred_element_type=F32)
         for d in range(1, nt):
-            stream += jnp.dot(flat[d, rows_at, :], ow[d - 1], preferred_element_type=F32)
+            stream += jnp.dot(flat[d, rows_at, :], ow[(t + nt - d) % nt], preferred_element_type=F32)
         center = stream - jnp.mean(stream, axis=-1, keepdims=True)
         spread = jnp.mean(center * center, axis=-1, keepdims=True)
         row = (center * lax.rsqrt(spread + 1e-05) * ngain[...]).astype(BF)
@@ -316,14 +335,17 @@
         lax.fori_loop(0, 2, body, 0)
 
     lifted[...] = lift(up0[...], 0)
+    ready("up", 1, 0, 1)
     lift_pair(1)
     for k in range(2, mid):
-        arrive(got_up)
-        got_up = ring(up0, up, k + 1)
+        issue("up", k + 1, 0)
+        if k + 1 < mid:
+            issue("up", k + 1, 1)
+        if k > 2:
+            issue("dn", k, 0, 1)
+        ready("up", k, 1)
         lift_pair(k)
-        arrive(got_dn)
-        got_dn = ring(dn0, dn, k + 1)
-    arrive(got_up)
+    ready("up", mid, 0)
     h = jnp.maximum(lifted[...] + lift(up[mid], mid), 0.0)
     hidden[...] = (h * h).astype(BF)
 
@@ -349,15 +371,20 @@
         out[:, pl.ds(pl.multiple_of(who * depth, depth), depth)] = y.astype(BF)
 
     lower(dn0[...], 0)
+    ready("dn", 1, 0, 1)
+    last = 0
     for k in range(1, mid):
-        lower(dn[k], k)
-        share(0 if k == 1 else n - k + 1)
-        lower(dn[n - k], n - k)
-        share(k)
-    share(mid + 1)
+        if k == mid - 1:
+            issue("dn", mid, 0)
+        ready("dn", k, 0, 1)
+        for slot in (k, n - k):
+            lower(dn[slot], slot)
+            share(last)
+            last = slot
+    share(last)
     for slot, group in waits[:-2]:
         finish(slot, group)
-    arrive(got_dn)
+    ready("dn", mid, 0)
     lower(dn[mid], mid)
     for slot, group in waits[-2:]:
         finish(slot, group)
@@ -377,36 +404,26 @@
     depth, units = up_weight.shape
     model = out_weight.shape[1]
     piece = residual.shape[0]
-    positions = (lax.axis_index("sp") * rows + jnp.arange(rows)).astype(F32)
     inverse = 10000.0 ** (-jnp.arange(0, half, dtype=F32) * 2.0 / head_width)
-    angle = positions[:, None] * inverse[None, :]
-    cosine, sine = jnp.cos(angle), jnp.sin(angle)
-    cosine = jnp.concatenate([cosine] * (2 * heads), axis=1)
-    sine = jnp.concatenate([-sine, sine] * heads, axis=1)
+    inverse = jnp.concatenate([inverse] * (2 * heads))[None, :]
     kv_width = 2 * width + heads * value_width
-    qm, kv0 = pl.pallas_call(
-        functools.partial(prep_kernel, heads),
-        out_shape=(
-            jax.ShapeDtypeStruct((2, heads * rows, width), BF),
-            jax.ShapeDtypeStruct((rows, kv_width), BF),
-        ),
-        name="prepare",
-    )(first_query, second_query, first_key, second_key, values, cosine, sine)
     vmem = pl.BlockSpec(memory_space=pltpu.VMEM)
     smem = pl.BlockSpec(memory_space=pltpu.SMEM)
     mid = n // 2
-    count = 2 * mid + 2 * (2 * mid - 1) + 2 * mid + 3 * (nt - 1) + n * (nt - 1)
+    count = 6 * (n - 1) + 3 * nt + (n + 1) * (nt - 1)
     maps = 2 * heads
     return pl.pallas_call(
         functools.partial(layer_kernel, n, nt, heads),
         out_shape=jax.ShapeDtypeStruct((piece, model), BF),
-        in_specs=[vmem, vmem, smem] + [vmem] * 6,
+        in_specs=[vmem] * 6 + [smem] + [vmem] * 6,
         out_specs=vmem,
         scratch_shapes=[
+            pltpu.VMEM((2, heads * rows, width), BF),
+            pltpu.VMEM((rows, kv_width), BF),
             pltpu.VMEM((n, rows, kv_width), BF),
             pltpu.VMEM((n, depth, units), BF),
             pltpu.VMEM((n, units, depth), BF),
-            pltpu.VMEM((nt - 1,) + out_weight.shape, BF),
+            pltpu.VMEM((nt,) + out_weight.shape, BF),
             pltpu.VMEM((nt, piece, model), BF),
             pltpu.VMEM((nt, rows, heads * value_width), BF),
             pltpu.VMEM((n, nt, piece, depth), BF),
@@ -425,7 +442,8 @@
             collective_id=0, has_side_effects=True, vmem_limit_bytes=60 * 2**20
         ),
         name="layer",
-    )(qm, kv0, lambdas, head_gain.reshape(-1, 1), out_weight, residual,
+    )(first_query, second_query, first_key, second_key, values, inverse,
+      lambdas, head_gain.reshape(1, -1), out_weight, residual,
       norm_gain.reshape(1, -1), up_weight, down_weight)
 
 
@@ -433,7 +451,7 @@
     n, nt = lax.axis_size("sp"), lax.axis_size("tp")
     gathered = n * sum(a.size * a.dtype.itemsize for a in (args[3], args[4], args[5], args[10], args[11]))
     gathered += nt * sum(a.size * a.dtype.itemsize for a in (args[0], args[8]))
-    if n % 2 == 0 and n >= 6 and 2 * gathered <= VMEM_BUDGET:
+    if n % 2 == 0 and n >= 6 and nt % 2 == 0 and 2 * gathered <= VMEM_BUDGET:
         return fused(n, nt, *args)
     return local(*args)
 

time: 127 us -> 114 us (0.90)
  Pallas kernels: 122 us -> 111 us
  local copies, waits for them, and re-layouts: 3.05 us -> 1.67 us
    pallas_call x1, Pallas kernels: 120 us -> 111 us  [fused(): pl.pallas_call(functools.partial(layer_kernel, n, nt, heads), out_shape=j...]
    pallas_call x1 -> x0, Pallas kernels: 2.14 us -> none  [fused(): pl.pallas_call(functools.partial(prep_kernel, heads), out_shape=(jax.Shap...]
where the time goes in v2:
time: 114 us
  Pallas kernels  111 us (97%)
  local copies, waits for them, and re-layouts  1.67 us (1%)
    pallas_call x1, Pallas kernels, fused(): pl.pallas_call(functools.partial(layer_kernel, n, nt, heads), out_shape=j...  111 us

profile of v2, /device:TPU:0, one launch (start us, length us, event | category | flops | bytes accessed | tf_op | source)
XLA Modules:
  0.0 113.7 jit_solution(17204451959694029689)
XLA Ops:
  0.0 0.6 maximum_bitcast_fusion.inverse
  0.6 111.4 %layer.1 = bf16[64,2048]{1,0:T(8,128)(2,1)} custom-call(bf16[256,128]{1,0:T(8,128)(2,1)} %qa.1, bf16[256,128]{1,0:T(8,128)(2,1)} %qb.1, bf16[256,128]{1,0:T(8,128)(2,1)} %ka.1, bf16[256,128]{1,0:T(8,128)(2,1)} %kb.1, bf16[256,256]{1,0:T(8,128)(2,1)} %v0.1, f32[1,128]{1,0:T(1,128)} %maximum_bitcast_fusion.inverse, f32[2]{0:T(128)} %lam.1, f32[1,128]{1,0:T(1,128)} %bitcast.5, ...), custom_call_target="tpu_custom_call" | custom-call | tf_op jit(solution)/shard_map/layer/pallas_call | solution.py:415
  112.0 1.7 %copy.14 = bf16[64,2048]{1,0:T(8,128)(2,1)} copy(bf16[64,2048]{1,0:T(8,128)(2,1)} %layer.1) | data formatting | bytes 524288
  (1 shorter events, 0.0 us)

commit v3 on v2

--- a/solution.py
+++ b/solution.py
@@ -2,6 +2,7 @@
 
 import jax
 import jax.numpy as jnp
+import numpy as np
 from jax import lax
 from jax.experimental import pallas as pl
 from jax.experimental.pallas import tpu as pltpu
@@ -141,7 +142,7 @@
     qa, qb, ka, kb, v0, inverse, lam, hgain, ow0, res0, ngain, up0, dn0,
     out,
     qm, kv0, kv, up, dn, ow, res, flat, normed, lifted, hidden, part, mine, got,
-    top, total, summed, send, recv,
+    top, total, summed, send, recv, load,
 ):
     s = lax.axis_index("sp")
     t = lax.axis_index("tp")
@@ -167,6 +168,12 @@
     right = {"sp": at_place(place + 1)}
     left = {"sp": at_place(place + n - 1)}
     mates = [{"tp": (t + d) % nt} for d in range(1, nt)]
+    loads = [
+        pltpu.make_async_copy(src, dst, load.at[i])
+        for i, (src, dst) in enumerate(((up0, up.at[0]), (dn0, dn.at[0]), (ow0, ow.at[t])))
+    ]
+    for c in loads:
+        c.start()
     barrier = pltpu.get_barrier_semaphore()
     for peer in [right, left] + mates:
         pl.semaphore_signal(barrier, inc=1, device_id=peer, device_id_type=pl.DeviceIdType.MESH)
@@ -289,6 +296,7 @@
     for filler in fillers:
         issue(*filler)
     ready("kv", mid, 0)
+    issue("dn", 2, 0, 1)
     absorb(kv[mid])
 
     for h in range(heads):
@@ -300,17 +308,18 @@
         flat[0, :, h * value_width : (h + 1) * value_width] = done.astype(BF)
 
     got_flat = [remote(flat.at[0], flat.at[d + 1], m) for d, m in enumerate(mates)]
-    issue("dn", 2, 0, 1)
     for d, pair in far:
         arrive(pair)
         there = (t + nt - d) % nt
         near += [remote(res.at[there], res.at[there], partner), remote(ow.at[there], ow.at[there], partner)]
     arrive(near + got_flat)
+    for c in loads:
+        c.wait()
 
     chunk = piece
     def norm_rows(q, carry):
         rows_at = pl.ds(pl.multiple_of(q * chunk, chunk), chunk)
-        stream = res[q].astype(F32) + jnp.dot(flat[0, rows_at, :], ow0[...], preferred_element_type=F32)
+        stream = res[q].astype(F32) + jnp.dot(flat[0, rows_at, :], ow[t], preferred_element_type=F32)
         for d in range(1, nt):
             stream += jnp.dot(flat[d, rows_at, :], ow[(t + nt - d) % nt], preferred_element_type=F32)
         center = stream - jnp.mean(stream, axis=-1, keepdims=True)
@@ -334,7 +343,7 @@
 
         lax.fori_loop(0, 2, body, 0)
 
-    lifted[...] = lift(up0[...], 0)
+    lifted[...] = lift(up[0], 0)
     ready("up", 1, 0, 1)
     lift_pair(1)
     for k in range(2, mid):
@@ -370,7 +379,7 @@
             y += got[slot, d].astype(F32)
         out[:, pl.ds(pl.multiple_of(who * depth, depth), depth)] = y.astype(BF)
 
-    lower(dn0[...], 0)
+    lower(dn[0], 0)
     ready("dn", 1, 0, 1)
     last = 0
     for k in range(1, mid):
@@ -404,18 +413,19 @@
     depth, units = up_weight.shape
     model = out_weight.shape[1]
     piece = residual.shape[0]
-    inverse = 10000.0 ** (-jnp.arange(0, half, dtype=F32) * 2.0 / head_width)
-    inverse = jnp.concatenate([inverse] * (2 * heads))[None, :]
+    inverse = 10000.0 ** (-np.arange(half) * 2.0 / head_width)
+    inverse = np.tile(inverse, 2 * heads)[None, :].astype(np.float32)
     kv_width = 2 * width + heads * value_width
     vmem = pl.BlockSpec(memory_space=pltpu.VMEM)
     smem = pl.BlockSpec(memory_space=pltpu.SMEM)
+    far = pl.BlockSpec(memory_space=pl.ANY)
     mid = n // 2
     count = 6 * (n - 1) + 3 * nt + (n + 1) * (nt - 1)
     maps = 2 * heads
     return pl.pallas_call(
         functools.partial(layer_kernel, n, nt, heads),
         out_shape=jax.ShapeDtypeStruct((piece, model), BF),
-        in_specs=[vmem] * 6 + [smem] + [vmem] * 6,
+        in_specs=[vmem] * 6 + [smem, vmem, far, vmem, vmem, far, far],
         out_specs=vmem,
         scratch_shapes=[
             pltpu.VMEM((2, heads * rows, width), BF),
@@ -437,6 +447,7 @@
             pltpu.VMEM((maps, value_width, rows), F32),
             pltpu.SemaphoreType.DMA((count,)),
             pltpu.SemaphoreType.DMA((count,)),
+            pltpu.SemaphoreType.DMA((3,)),
         ],
         compiler_params=pltpu.CompilerParams(
             collective_id=0, has_side_effects=True, vmem_limit_bytes=60 * 2**20

time: 114 us -> 113 us (level)
  no operation moved by 1% of the time
where the time goes in v3:
time: 113 us
  Pallas kernels  111 us (98%)
  local copies, waits for them, and re-layouts  1.67 us (1%)
    pallas_call x1, Pallas kernels, fused(): pl.pallas_call(functools.partial(layer_kernel, n, nt, heads), out_shape=j...  111 us

profile of v3, /device:TPU:0, one launch (start us, length us, event | category | flops | bytes accessed | tf_op | source)
XLA Modules:
  0.0 112.6 jit_solution(14284151977713583202)
XLA Ops:
  0.0 111.0 %layer.1 = bf16[64,2048]{1,0:T(8,128)(2,1)} custom-call(bf16[256,128]{1,0:T(8,128)(2,1)} %qa.1, bf16[256,128]{1,0:T(8,128)(2,1)} %qb.1, bf16[256,128]{1,0:T(8,128)(2,1)} %ka.1, bf16[256,128]{1,0:T(8,128)(2,1)} %kb.1, bf16[256,256]{1,0:T(8,128)(2,1)} %v0.1, f32[1,128]{1,0:T(1,128)} %constant.2.clone.inverse, f32[2]{0:T(128)} %lam.1, f32[1,128]{1,0:T(1,128)} %bitcast.3, ...), custom_call_target="tpu_custom_call" | custom-call | tf_op jit(solution)/shard_map/layer/pallas_call | solution.py:425
  111.0 1.7 %copy.15 = bf16[64,2048]{1,0:T(8,128)(2,1)} copy(bf16[64,2048]{1,0:T(8,128)(2,1)} %layer.1) | data formatting | bytes 524288

commit v4 on v3

--- a/solution.py
+++ b/solution.py
@@ -139,10 +139,10 @@
 
 def layer_kernel(
     n, nt, heads,
-    qa, qb, ka, kb, v0, inverse, lam, hgain, ow0, res0, ngain, up0, dn0,
+    qa_far, qb_far, ka_far, kb_far, v_far, inverse, lam, hgain, ow0, res0, ngain, up0, dn0,
     out,
     qm, kv0, kv, up, dn, ow, res, flat, normed, lifted, hidden, part, mine, got,
-    top, total, summed, send, recv, load,
+    top, total, summed, send, recv, load, qa, qb, ka, kb,
 ):
     s = lax.axis_index("sp")
     t = lax.axis_index("tp")
@@ -172,7 +172,14 @@
         pltpu.make_async_copy(src, dst, load.at[i])
         for i, (src, dst) in enumerate(((up0, up.at[0]), (dn0, dn.at[0]), (ow0, ow.at[t])))
     ]
-    for c in loads:
+    entries = [
+        pltpu.make_async_copy(src, dst, load.at[3 + i])
+        for i, (src, dst) in enumerate((
+            (ka_far, ka), (kb_far, kb), (v_far, kv0.at[:, pl.ds(2 * width, v_far.shape[1])]),
+            (qa_far, qa), (qb_far, qb),
+        ))
+    ]
+    for c in entries + loads:
         c.start()
     barrier = pltpu.get_barrier_semaphore()
     for peer in [right, left] + mates:
@@ -269,7 +276,8 @@
         other = jnp.where(low, pltpu.roll(x, width - half, 1), pltpu.roll(x, half, 1))
         return x * cos + other * sin
 
-    kv0[:, 2 * width :] = v0[...]
+    for c in entries:
+        c.wait()
     kv0[:, :width] = turn(ka).astype(BF)
     kv0[:, width : 2 * width] = turn(kb).astype(BF)
     for which, ref in enumerate((qa, qb)):
@@ -425,7 +433,7 @@
     return pl.pallas_call(
         functools.partial(layer_kernel, n, nt, heads),
         out_shape=jax.ShapeDtypeStruct((piece, model), BF),
-        in_specs=[vmem] * 6 + [smem, vmem, far, vmem, vmem, far, far],
+        in_specs=[far] * 5 + [vmem, smem, vmem, far, vmem, vmem, far, far],
         out_specs=vmem,
         scratch_shapes=[
             pltpu.VMEM((2, heads * rows, width), BF),
@@ -447,8 +455,8 @@
             pltpu.VMEM((maps, value_width, rows), F32),
             pltpu.SemaphoreType.DMA((count,)),
             pltpu.SemaphoreType.DMA((count,)),
-            pltpu.SemaphoreType.DMA((3,)),
-        ],
+            pltpu.SemaphoreType.DMA((8,)),
+        ] + [pltpu.VMEM((rows, width), BF)] * 4,
         compiler_params=pltpu.CompilerParams(
             collective_id=0, has_side_effects=True, vmem_limit_bytes=60 * 2**20
         ),

time: 113 us -> 113 us (level)
  no operation moved by 1% of the time
where the time goes in v4:
time: 113 us
  Pallas kernels  111 us (98%)
  local copies, waits for them, and re-layouts  1.67 us (1%)
    pallas_call x1, Pallas kernels, fused(): pl.pallas_call(functools.partial(layer_kernel, n, nt, heads), out_shape=j...  111 us

profile of v4, /device:TPU:0, one launch (start us, length us, event | category | flops | bytes accessed | tf_op | source)
XLA Modules:
  0.0 112.5 jit_solution(12787389020220801517)
XLA Ops:
  0.0 110.9 %layer.1 = bf16[64,2048]{1,0:T(8,128)(2,1)} custom-call(bf16[256,128]{1,0:T(8,128)(2,1)} %qa_far.1, bf16[256,128]{1,0:T(8,128)(2,1)} %qb_far.1, bf16[256,128]{1,0:T(8,128)(2,1)} %ka_far.1, bf16[256,128]{1,0:T(8,128)(2,1)} %kb_far.1, bf16[256,256]{1,0:T(8,128)(2,1)} %v_far.1, f32[1,128]{1,0:T(1,128)} %constant.2.clone.inverse, f32[2]{0:T(128)} %lam.1, ...), custom_call_target="tpu_custom_call" | custom-call | tf_op jit(solution)/shard_map/layer/pallas_call | solution.py:433
  110.9 1.7 %copy.15 = bf16[64,2048]{1,0:T(8,128)(2,1)} copy(bf16[64,2048]{1,0:T(8,128)(2,1)} %layer.1) | data formatting | bytes 524288
